TPU v7x, 32 devices: a whole 2x2x4 slice. The times are simulated.
32 devices in a mesh: fs: 8 (over z, y), tp: 4 (over x, core).
Axes of the slice: x: 2, y: 2, z: 4, core: 2. Of those that a mesh axis runs over, the one named last changes fastest.
Arguments:
- inputs: bfloat16 [4608, 2048], P('fs'), may hold values from -6 to 6
- query_cotangent: bfloat16 [4608, 1024], P('fs', 'tp'), may hold values from -0.017944336 to 0.017944336
- value_cotangent: bfloat16 [4608, 1024], P('fs', 'tp'), may hold values from -0.017944336 to 0.017944336
- weights_query: float32 [2048, 1024], P('fs', 'tp'), may hold values from -6 to 6
- weights_value: float32 [2048, 1024], P('fs', 'tp'), may hold values from -6 to 6
- basis_query: bfloat16 [1024, 32], P('tp'), may hold values from -0.75 to 0.75
- basis_value: bfloat16 [1024, 32], P('tp'), may hold values from -0.75 to 0.75
- first_query: float32 [2048, 512], P('fs', 'tp'), may hold values from -5.4 to 5.4, as said below
- second_query: float32 [2048, 512], P('fs', 'tp'), may hold values from 0.05 to 1
- first_value: float32 [2048, 512], P('fs', 'tp'), may hold values from -5.4 to 5.4, as said below
- second_value: float32 [2048, 512], P('fs', 'tp'), may hold values from 0.05 to 1
Outputs:
- step_query: float32 [2048, 1024], P('fs', 'tp')
- step_value: float32 [2048, 1024], P('fs', 'tp')
- new_query: float32 [2048, 1024], P('fs', 'tp')
- new_value: float32 [2048, 1024], P('fs', 'tp')
- copy_query: bfloat16 [2048, 1024], P(None, 'tp')
- copy_value: bfloat16 [2048, 1024], P(None, 'tp')
- moment_query: float32 [2048, 512], P('fs', 'tp')
- square_query: float32 [2048, 512], P('fs', 'tp')
- moment_value: float32 [2048, 512], P('fs', 'tp')
- square_value: float32 [2048, 512], P('fs', 'tp')
Inputs may be any that keep to these rules, and one draw needn't show every extreme that they name: `first_query`: first moments, with a spread of scale from row to row. `first_value`: first moments, with a spread of scale from row to row.
All inputs are finite; a program needn't handle non-finite values.
Results may differ from a plain program's by a relative error of at most 0.003.
Values may be sent and summed in bfloat16 or wider, within the bound.
A program may use at most 64 MiB of HBM per device.

v0:
```python
import jax
import jax.numpy as jnp
from jax import lax
from jax.sharding import PartitionSpec as P

D = 2048
HEADS = 16
HEAD = 64
RK = 32


def from_space(direction, factor, heads_here):
    count = direction.shape[0]
    split = direction.reshape(count, heads_here, RK)
    out = jnp.einsum("nhr,hdr->nhd", split, factor, precision=lax.Precision.HIGHEST)
    return out.reshape(count, heads_here * HEAD)


def moments(reduced, first, second):
    moment = 0.9 * first + 0.1 * reduced
    square = 0.95 * second + 0.05 * reduced * reduced
    direction = moment / (jnp.sqrt(square) + 1e-08)
    return (moment, square, direction)


def per_device(
    inputs,
    query_cotangent,
    value_cotangent,
    weights_query,
    weights_value,
    basis_query,
    basis_value,
    first_query,
    second_query,
    first_value,
    second_value,
):
    own_cols = weights_query.shape[1]
    heads_here = own_cols // HEAD
    space_cols = heads_here * RK
    factor_q = basis_query.reshape(heads_here, HEAD, RK).astype(jnp.float32)
    factor_v = basis_value.reshape(heads_here, HEAD, RK).astype(jnp.float32)
    contract = (((0,), (0,)), ((), ()))
    tok_count = query_cotangent.shape[0]
    bf_q = basis_query.reshape(heads_here, HEAD, RK)
    bf_v = basis_value.reshape(heads_here, HEAD, RK)
    small_q = jnp.einsum(
        "thd,hdr->thr",
        query_cotangent.reshape(tok_count, heads_here, HEAD),
        bf_q,
        preferred_element_type=jnp.float32,
    )
    small_v = jnp.einsum(
        "thd,hdr->thr",
        value_cotangent.reshape(tok_count, heads_here, HEAD),
        bf_v,
        preferred_element_type=jnp.float32,
    )
    small_both = jnp.concatenate(
        (small_q.reshape(tok_count, space_cols), small_v.reshape(tok_count, space_cols)), axis=1
    )
    upper_part = small_both.astype(jnp.bfloat16)
    lower_part = (small_both - upper_part.astype(jnp.float32)).astype(jnp.bfloat16)
    high = lax.dot_general(inputs, upper_part, contract, preferred_element_type=jnp.float32)
    reduced = lax.psum_scatter(
        high + lax.dot_general(inputs, lower_part, contract, preferred_element_type=jnp.float32),
        "fs",
        scatter_dimension=0,
        tiled=True,
    )
    reduced_q = reduced[:, :space_cols]
    reduced_v = reduced[:, space_cols:]
    moment_q, square_q, direction_q = moments(reduced_q, first_query, second_query)
    moment_v, square_v, direction_v = moments(reduced_v, first_value, second_value)
    total_q, total_v = lax.psum(
        (jnp.sum(direction_q * direction_q), jnp.sum(direction_v * direction_v)), ("fs", "tp")
    )
    entries = D * HEADS * RK
    scale_q = 1.0 / jnp.sqrt(total_q / entries + 0.25)
    scale_v = 1.0 / jnp.sqrt(total_v / entries + 0.25)
    step_q = scale_q * from_space(direction_q, factor_q, heads_here)
    step_v = scale_v * from_space(direction_v, factor_v, heads_here)
    fresh_q = weights_query - 0.1 * step_q
    fresh_v = weights_value - 0.1 * step_v
    copy_q, copy_v = (
        lax.all_gather(fresh_q.astype(jnp.bfloat16), "fs", axis=0, tiled=True),
        lax.all_gather(fresh_v.astype(jnp.bfloat16), "fs", axis=0, tiled=True),
    )
    return (
        step_q,
        step_v,
        fresh_q,
        fresh_v,
        copy_q,
        copy_v,
        moment_q,
        square_q,
        moment_v,
        square_v,
    )


def solution(mesh):
    placed = (
        P("fs", None),
        P("fs", "tp"),
        P("fs", "tp"),
        P("fs", "tp"),
        P("fs", "tp"),
        P("tp", None),
        P("tp", None),
        P("fs", "tp"),
        P("fs", "tp"),
        P("fs", "tp"),
        P("fs", "tp"),
    )
    return jax.shard_map(
        per_device,
        mesh=mesh,
        in_specs=placed,
        out_specs=(
            P("fs", "tp"),
            P("fs", "tp"),
            P("fs", "tp"),
            P("fs", "tp"),
            P(None, "tp"),
            P(None, "tp"),
            P("fs", "tp"),
            P("fs", "tp"),
            P("fs", "tp"),
            P("fs", "tp"),
        ),
        check_vma=False,
    )
```

profile of v0, /device:TPU:0, one launch (start us, length us, event | category | flops | bytes accessed | tf_op | source)
XLA Modules:
  0.0 223.8 jit_solution(16746739006652718097)
XLA Ops:
  7.2 0.0 copy-start
  7.2 0.0 reduce-scatter.2.cloned.1.call-start
  7.2 1.0 reshape.52
  8.2 0.0 copy-start.4
  8.2 0.8 reshape.55
  9.0 1.2 copy.40
  10.2 1.2 copy.42
  11.4 0.2 fusion.10
  11.6 0.2 fusion.7
  11.7 0.0 copy-done
  11.8 1.0 fusion.2
  12.8 0.0 copy-done.4
  12.8 0.0 copy-start.5
  12.8 2.3 %fusion = f32[2048,256]{0,1:T(8,128)} fusion(f32[256,2048]{1,0:T(8,128)S(1)} %fusion.2, bf16[576,2048]{1,0:T(8,128)(2,1)S(1)} %copy-done, f32[576,128]{0,1:T(8,128)S(1)} %bitcast.31, f32[576,128]{0,1:T(8,128)S(1)} %bitcast.29), kind=kOutput, calls=%fused_computation.1 | convolution fusion | flops 605241344 | bytes 7143424 | tf_op jit(solution)/shard_map/dot_general | solution.py:67
  15.1 0.0 copy-start.6
  15.1 0.0 copy-start.7
  15.1 0.0 copy-start.8
  15.1 0.0 reduce-scatter.2.cloned.1.call-update
  15.2 0.0 all-gather.5.cloned.1.call-start
  15.2 0.0 copy-done.5
  15.2 0.1 copy.39
  15.3 0.7 copy-done.6
  16.0 0.1 copy.44
  16.1 0.0 copy-done.7
  16.1 0.1 copy.46
  16.3 0.0 copy-done.8
  16.3 0.1 copy.47
  16.4 70.6 %reduce-scatter.2.cloned.1.call-done = f32[256,256]{0,1:T(8,128)} async-done(((f32[2048,256]{0,1:T(8,128)}), f32[256,256]{0,1:T(8,128)}) %reduce-scatter.2.cloned.1.call-update) | async-done | bytes 262160 | tf_op jit(solution)/shard_map/reduce_scatter | solution.py:66
  86.9 2.4 %multiply_reduce_fusion = (f32[]{:T(128)}, f32[256,128]{0,1:T(8,128)S(1)}, f32[256,128]{0,1:T(8,128)}, f32[256,128]{0,1:T(8,128)S(1)}, f32[]{:T(128)}, /*index=5...) fusion(f32[256,256]{0,1:T(8,128)} %reduce-scatter.2.cloned.1.call-done, f32[256,128]{0,1:T(8,128)S(1)} %copy.47, ...), kind=kLoop, calls=%fused_computation.14 | loop fusion | flops 720894 | bytes 1572872 | tf_op jit(solution)/shard_map/reduce_sum | solution.py:77
  89.3 39.8 %all-reduce = (f32[]{:T(128)}, f32[]{:T(128)}) all-reduce(f32[]{:T(128)} %get-tuple-element.44, f32[]{:T(128)} %get-tuple-element.36), channel_id=1, replica_groups=mesh['fs'=8,'tp'=4] {'fs','tp'}, use_global_device_ids=true, to_apply=%region_2.0 | all-reduce | flops 2 | bytes 16 | tf_op jit(solution)/shard_map/psum | solution.py:76
  129.8 0.3 convolution_multiply_fusion
  130.1 0.1 copy.52
  130.3 0.0 copy-start.1
  130.3 1.8 fusion.14
  132.1 0.0 all-gather.5.cloned.1.call-update
  132.1 0.0 all-gather.3.cloned.1.call-start
  132.9 1.2 convolution_multiply_fusion.1
  134.1 0.1 copy.51
  134.2 0.0 copy-start.2
  134.2 1.8 fusion.15
  136.1 0.0 all-gather.3.cloned.1.call-update
  136.1 1.7 copy.56
  137.8 0.8 copy.55
  138.5 0.8 copy.54
  139.3 0.8 copy.53
  140.0 32.2 %all-gather.5.cloned.1.call-done = bf16[2048,256]{1,0:T(8,128)(2,1)} async-done(((bf16[256,256]{1,0:T(8,128)(2,1)}), bf16[2048,256]{1,0:T(8,128)(2,1)}) %all-gather.5.cloned.1.call-update) | async-done | bytes 1048592 | tf_op jit(solution)/shard_map/all_gather | solution.py:88
  172.3 41.7 %all-gather.3.cloned.1.call-done = bf16[2048,256]{1,0:T(8,128)(2,1)} async-done(((bf16[256,256]{1,0:T(8,128)(2,1)}), bf16[2048,256]{1,0:T(8,128)(2,1)}) %all-gather.3.cloned.1.call-update) | async-done | bytes 1048592 | tf_op jit(solution)/shard_map/all_gather | solution.py:87
  214.0 0.0 copy-start.3
  214.0 2.4 %copy.67 = bf16[2048,256]{1,0:T(8,128)(2,1)} copy(bf16[2048,256]{1,0:T(8,128)(2,1)} %all-gather.3.cloned.1.call-done) | data formatting | bytes 2097152
  216.3 0.0 copy-done.1
  216.3 0.0 copy-done.3
  216.3 1.0 copy.68
  217.3 0.0 copy-done.2
Async XLA Ops:
  7.2 4.6 %copy-start = (bf16[576,2048]{1,0:T(8,128)(2,1)S(1)}, bf16[576,2048]{1,0:T(8,128)(2,1)}, u32[]{:S(2)}) copy-start(bf16[576,2048]{1,0:T(8,128)(2,1)} %param.11) | copy-start | bytes 7077892
  7.2 79.7 %reduce-scatter.2.cloned.1.call-start = ((), (), s32[]{:S(2)}) async-start(), calls=%async_computation.1 | async-start | bytes 2359296 | tf_op jit(solution)/shard_map/reduce_scatter | solution.py:66
  8.2 4.6 %copy-start.4 = (bf16[4,64,32]{1,0,2:T(4,128)(2,1)}, bf16[4,64,32]{1,0,2:T(4,128)(2,1)S(1)}, u32[]{:S(2)}) copy-start(bf16[4,64,32]{1,0,2:T(4,128)(2,1)S(1)} %reshape.52) | copy-start | bytes 49156
  12.8 2.4 %copy-start.5 = (f32[256,128]{1,0:T(8,128)S(1)}, f32[256,128]{1,0:T(8,128)}, u32[]{:S(2)}) copy-start(f32[256,128]{1,0:T(8,128)} %param.18) | copy-start | bytes 393220
  15.1 0.9 copy-start.6
  15.1 1.0 copy-start.7
  15.1 1.1 copy-start.8
  15.2 157.1 %all-gather.5.cloned.1.call-start = ((), (), s32[]{:S(2)}) async-start(), calls=%async_computation.3 | async-start | bytes 1179648 | tf_op jit(solution)/shard_map/all_gather | solution.py:88
  130.3 86.1 %copy-start.1 = (f32[256,256]{1,0:T(8,128)}, f32[256,256]{1,0:T(8,128)S(1)}, u32[]{:S(2)}) copy-start(f32[256,256]{1,0:T(8,128)S(1)} %copy.52) | copy-start | bytes 786436
  132.1 81.8 %all-gather.3.cloned.1.call-start = ((), (), s32[]{:S(2)}) async-start(), calls=%async_computation.2 | async-start | bytes 1179648 | tf_op jit(solution)/shard_map/all_gather | solution.py:87
  134.2 83.1 %copy-start.2 = (f32[256,256]{1,0:T(8,128)}, f32[256,256]{1,0:T(8,128)S(1)}, u32[]{:S(2)}) copy-start(f32[256,256]{1,0:T(8,128)S(1)} %copy.51) | copy-start | bytes 786436
  214.0 2.4 %copy-start.3 = (bf16[2048,256]{1,0:T(8,128)(2,1)S(1)}, bf16[2048,256]{1,0:T(8,128)(2,1)}, u32[]{:S(2)}) copy-start(bf16[2048,256]{1,0:T(8,128)(2,1)} %all-gather.5.cloned.1.call-done) | copy-start | bytes 3145732
Sparse Core Ops, SparseCore 0:
  15.3 71.6 reduce-scatter.1
  132.3 39.9 all-gather.4
  175.0 38.9 all-gather.2
where the time goes:
time: 224 us
  waiting for transfers between devices  145 us (65%)
  blocking collectives  39.8 us (18%)
  between operations  15.3 us (7%)
  local copies, waits for them, and re-layouts  12.7 us (6%)
  other arithmetic  6.06 us (3%)
  matrix products  5.25 us (2%)
    reduce_scatter x1, waiting for transfers between devices, per_device(): lax.psum_scatter(high + lax.dot_general(inputs, lower_part, contract, pre...  70.6 us
    all_gather x1, waiting for transfers between devices, per_device(): lax.all_gather(fresh_q.astype(jnp.bfloat16), 'fs', axis=0, tiled=True)  41.7 us
    psum x1, blocking collectives, per_device(): lax.psum((jnp.sum(direction_q * direction_q), jnp.sum(direction_v * direc...  39.8 us
    all_gather x1, waiting for transfers between devices, per_device(): lax.all_gather(fresh_v.astype(jnp.bfloat16), 'fs', axis=0, tiled=True)  32.2 us
    unnamed x32, local copies, waits for them, and re-layouts  11 us
  transfers between devices with their start and end apart: 3, of which 3 were waited for; matrix products, arithmetic and copies ran while one was open for 3% of the time, Pallas kernels for 0%

commit v1 on v0

--- a/solution.py
+++ b/solution.py
@@ -7,6 +7,18 @@
 HEADS = 16
 HEAD = 64
 RK = 32
+
+
+def collect(shard, axis, dim):
+    ways, here, turn = (lax.axis_size(axis), lax.axis_index(axis), shard.shape[dim])
+    shape = [n * ways if d == dim else n for d, n in enumerate(shard.shape)]
+    full = lax.dynamic_update_slice_in_dim(
+        jnp.zeros(shape, shard.dtype), shard, here * turn, axis=dim
+    )
+    for far in range(1, ways):
+        shard = lax.ppermute(shard, axis, [(d, (d + 1) % ways) for d in range(ways)])
+        full = lax.dynamic_update_slice_in_dim(full, shard, (here - far) % ways * turn, axis=dim)
+    return full
 
 
 def from_space(direction, factor, heads_here):
@@ -84,7 +96,7 @@
     fresh_q = weights_query - 0.1 * step_q
     fresh_v = weights_value - 0.1 * step_v
     copy_q, copy_v = (
-        lax.all_gather(fresh_q.astype(jnp.bfloat16), "fs", axis=0, tiled=True),
+        collect(fresh_q.astype(jnp.bfloat16), "fs", 0),
         lax.all_gather(fresh_v.astype(jnp.bfloat16), "fs", axis=0, tiled=True),
     )
     return (

time: 224 us -> 205 us (0.915)
  waiting for transfers between devices: 145 us -> 114 us
  local copies, waits for them, and re-layouts: 12.7 us -> 19.8 us
  starting transfers between devices: 0.12 us -> 3.72 us
    ppermute x0 -> x7, waiting for transfers between devices: none -> 43.1 us  [collect(): lax.ppermute(shard, axis, [(d, (d + 1) % ways) for d in range(ways)])]
    all_gather x1 -> x0, waiting for transfers between devices: 41.7 us -> none  [per_device(): lax.all_gather(fresh_q.astype(jnp.bfloat16), 'fs', axis=0, tiled=True)]
    all_gather x1, waiting for transfers between devices: 32.2 us -> 0.01 us  [per_device(): lax.all_gather(fresh_v.astype(jnp.bfloat16), 'fs', axis=0, tiled=True)]
    dynamic_update_slice x0 -> x7, local copies, waits for them, and re-layouts: none -> 7.36 us  [collect(): lax.dynamic_update_slice_in_dim(full, shard, (here - far) % ways * turn,...]
    ppermute x0 -> x7, starting transfers between devices: none -> 3.64 us  [collect(): lax.ppermute(shard, axis, [(d, (d + 1) % ways) for d in range(ways)])]
    unnamed x32 -> x35, local copies, waits for them, and re-layouts: 11 us -> 9.67 us
  transfers between devices with their start and end apart: 3 -> 9, of which waited for: 3 -> 8; matrix products, arithmetic and copies ran while one was open for 3% -> 7% of each run, Pallas kernels for 0% -> 0%
where the time goes in v1:
time: 205 us
  waiting for transfers between devices  114 us (56%)
  blocking collectives  39.8 us (19%)
  local copies, waits for them, and re-layouts  19.8 us (10%)
  between operations  15.6 us (8%)
  other arithmetic  5.93 us (3%)
  matrix products  5.84 us (3%)
  starting transfers between devices  3.72 us (2%)
    reduce_scatter x1, waiting for transfers between devices, per_device(): lax.psum_scatter(high + lax.dot_general(inputs, lower_part, contract, pre...  70.9 us
    ppermute x7, waiting for transfers between devices, collect(): lax.ppermute(shard, axis, [(d, (d + 1) % ways) for d in range(ways)])  43.1 us
    psum x1, blocking collectives, per_device(): lax.psum((jnp.sum(direction_q * direction_q), jnp.sum(direction_v * direc...  39.8 us
    unnamed x35, local copies, waits for them, and re-layouts  9.67 us
    dynamic_update_slice x7, local copies, waits for them, and re-layouts, collect(): lax.dynamic_update_slice_in_dim(full, shard, (here - far) % ways * turn,...  7.36 us
  transfers between devices with their start and end apart: 9, of which 8 were waited for; matrix products, arithmetic and copies ran while one was open for 7% of the time, Pallas kernels for 0%

profile of v1, /device:TPU:0, one launch (start us, length us, event | category | flops | bytes accessed | tf_op | source)
XLA Modules:
  0.0 204.8 jit_solution(6709640932893115765)
XLA Ops:
  7.2 0.0 copy-start
  7.2 0.0 reduce-scatter.2.cloned.1.call-start
  7.2 1.0 reshape.52
  8.2 0.0 copy-start.4
  8.2 0.8 reshape.55
  9.0 0.0 copy-start.5
  9.0 1.2 copy.40
  10.2 1.2 copy.42
  11.4 0.2 fusion.10
  11.6 0.2 fusion.7
  11.8 1.0 fusion.2
  12.8 0.0 copy-start.6
  12.8 2.3 %fusion = f32[2048,256]{0,1:T(8,128)} fusion(f32[256,2048]{1,0:T(8,128)S(1)} %fusion.2, bf16[576,2048]{1,0:T(8,128)(2,1)S(1)} %copy-done, f32[576,128]{0,1:T(8,128)S(1)} %bitcast.31, f32[576,128]{0,1:T(8,128)S(1)} %bitcast.29), kind=kOutput, calls=%fused_computation.1 | convolution fusion | flops 605241344 | bytes 7143424 | tf_op jit(solution)/shard_map/dot_general | solution.py:79
  15.1 0.0 copy-done.4
  15.1 0.0 copy-start.9
  15.2 0.0 reduce-scatter.2.cloned.1.call-update
  15.2 0.0 all-gather.2.cloned.1.call-start
  15.2 0.1 copy.39
  15.3 0.7 copy-done.7
  16.0 0.1 copy.44
  16.2 0.1 copy.46
  16.3 0.0 copy-done.9
  16.3 0.1 copy.47
  16.4 70.9 %reduce-scatter.2.cloned.1.call-done = f32[256,256]{0,1:T(8,128)} async-done(((f32[2048,256]{0,1:T(8,128)}), f32[256,256]{0,1:T(8,128)}) %reduce-scatter.2.cloned.1.call-update) | async-done | bytes 262160 | tf_op jit(solution)/shard_map/reduce_scatter | solution.py:78
  87.3 2.4 %multiply_reduce_fusion = (f32[]{:T(128)}, f32[256,128]{0,1:T(8,128)S(1)}, f32[256,128]{0,1:T(8,128)}, f32[256,128]{0,1:T(8,128)S(1)}, f32[]{:T(128)}, /*index=5...) fusion(f32[256,256]{0,1:T(8,128)} %reduce-scatter.2.cloned.1.call-done, f32[256,128]{0,1:T(8,128)S(1)} %copy.47, ...), kind=kLoop, calls=%fused_computation.14 | loop fusion | flops 720894 | bytes 1572872 | tf_op jit(solution)/shard_map/reduce_sum | solution.py:89
  89.6 39.8 %all-reduce = (f32[]{:T(128)}, f32[]{:T(128)}) all-reduce(f32[]{:T(128)} %get-tuple-element.45, f32[]{:T(128)} %get-tuple-element.37), channel_id=1, replica_groups=mesh['fs'=8,'tp'=4] {'fs','tp'}, use_global_device_ids=true, to_apply=%region_2.0 | all-reduce | flops 2 | bytes 16 | tf_op jit(solution)/shard_map/psum | solution.py:88
  130.2 1.1 convolution_multiply_fusion
  131.2 0.1 copy.52
  131.4 0.0 copy-start.1
  131.4 1.8 fusion.14
  133.2 0.0 all-gather.2.cloned.1.call-update
  133.9 1.1 convolution_multiply_fusion.1
  135.0 0.1 copy.51
  135.1 0.0 copy-start.2
  135.1 0.0 copy-start.3
  135.2 1.0 broadcast_in_dim.3
  136.2 1.7 constant_dynamic-update-slice_fusion.7
  137.9 2.5 %collective-permute-start = (bf16[256,256]{1,0:T(8,128)(2,1)S(1)}, bf16[256,256]{1,0:T(8,128)(2,1)S(1)}, u32[]{:S(2)}, u32[]{:S(2)}) collective-permute-start(bf16[256,256]{1,0:T(8,128)(2,1)S(1)} %get-tuple-element.35), channel_id=1, source_target_pairs={{0,4},{4,8},{8,12},{12,16},{16,20},{20,24},{24,28},{28,0},{1,5},{5... | collective-permute-start | bytes 393224 | tf_op jit(solution)/shard_map/ppermute | solution.py:19
  140.4 5.3 %collective-permute-done = bf16[256,256]{1,0:T(8,128)(2,1)S(1)} collective-permute-done((bf16[256,256]{1,0:T(8,128)(2,1)S(1)}, bf16[256,256]{1,0:T(8,128)(2,1)S(1)}, u32[]{:S(2)}, u32[]{:S(2)}) %collective-permute-start) | collective-permute-done | bytes 131104 | tf_op jit(solution)/shard_map/ppermute | solution.py:19
  145.7 1.2 collective-permute-start.1
  146.9 7.1 %collective-permute-done.1 = bf16[256,256]{1,0:T(8,128)(2,1)S(1)} collective-permute-done((bf16[256,256]{1,0:T(8,128)(2,1)S(1)}, bf16[256,256]{1,0:T(8,128)(2,1)S(1)}, u32[]{:S(2)}, u32[]{:S(2)}) %collective-permute-start.1) | collective-permute-done | bytes 131104 | tf_op jit(solution)/shard_map/ppermute | solution.py:19
  154.0 0.7 copy-done.10
  154.6 0.0 collective-permute-start.2
  154.6 7.9 %collective-permute-done.2 = bf16[256,256]{1,0:T(8,128)(2,1)} collective-permute-done((bf16[256,256]{1,0:T(8,128)(2,1)S(1)}, bf16[256,256]{1,0:T(8,128)(2,1)}, u32[]{:S(2)}, u32[]{:S(2)}) %collective-permute-start.2) | collective-permute-done | bytes 131104 | tf_op jit(solution)/shard_map/ppermute | solution.py:19
  162.5 0.0 collective-permute-start.3
  162.5 0.8 copy.56
  163.3 0.8 copy.55
  164.0 0.8 copy.54
  164.8 0.8 copy.53
  165.5 6.3 %collective-permute-done.3 = bf16[256,256]{1,0:T(8,128)(2,1)} collective-permute-done((bf16[256,256]{1,0:T(8,128)(2,1)}, bf16[256,256]{1,0:T(8,128)(2,1)}, u32[]{:S(2)}, u32[]{:S(2)}) %collective-permute-start.3) | collective-permute-done | bytes 131104 | tf_op jit(solution)/shard_map/ppermute | solution.py:19
  171.8 0.0 collective-permute-start.4
  171.8 0.7 constant_dynamic-update-slice_fusion.6
  172.5 1.6 constant_dynamic-update-slice_fusion.5
  174.1 5.6 %collective-permute-done.4 = bf16[256,256]{1,0:T(8,128)(2,1)S(1)} collective-permute-done((bf16[256,256]{1,0:T(8,128)(2,1)}, bf16[256,256]{1,0:T(8,128)(2,1)S(1)}, u32[]{:S(2)}, u32[]{:S(2)}) %collective-permute-start.4) | collective-permute-done | bytes 131104 | tf_op jit(solution)/shard_map/ppermute | solution.py:19
  179.7 0.0 collective-permute-start.5
  179.7 1.6 constant_dynamic-update-slice_fusion.4
  181.3 1.6 constant_dynamic-update-slice_fusion.3
  182.9 4.5 %collective-permute-done.5 = bf16[256,256]{1,0:T(8,128)(2,1)S(1)} collective-permute-done((bf16[256,256]{1,0:T(8,128)(2,1)S(1)}, bf16[256,256]{1,0:T(8,128)(2,1)S(1)}, u32[]{:S(2)}, u32[]{:S(2)}) %collective-permute-start.5) | collective-permute-done | bytes 131104 | tf_op jit(solution)/shard_map/ppermute | solution.py:19
  187.4 0.0 collective-permute-start.6
  187.4 0.7 constant_dynamic-update-slice_fusion.2
  188.1 0.7 constant_dynamic-update-slice_fusion.1
  188.7 6.3 %collective-permute-done.6 = bf16[256,256]{1,0:T(8,128)(2,1)S(1)} collective-permute-done((bf16[256,256]{1,0:T(8,128)(2,1)S(1)}, bf16[256,256]{1,0:T(8,128)(2,1)S(1)}, u32[]{:S(2)}, u32[]{:S(2)}) %collective-permute-start.6) | collective-permute-done | bytes 131104 | tf_op jit(solution)/shard_map/ppermute | solution.py:19
  195.1 0.7 constant_dynamic-update-slice_fusion
  195.7 2.3 %copy.74 = bf16[2048,256]{1,0:T(8,128)(2,1)} copy(bf16[2048,256]{1,0:T(8,128)(2,1)} %all-gather.2.cloned.1.call-done) | data formatting | bytes 2097152
  (11 shorter events, 0.0 us)
Async XLA Ops:
  7.2 4.6 %copy-start = (bf16[576,2048]{1,0:T(8,128)(2,1)S(1)}, bf16[576,2048]{1,0:T(8,128)(2,1)}, u32[]{:S(2)}) copy-start(bf16[576,2048]{1,0:T(8,128)(2,1)} %param.11) | copy-start | bytes 7077892
  7.2 80.1 %reduce-scatter.2.cloned.1.call-start = ((), (), s32[]{:S(2)}) async-start(), calls=%async_computation.1 | async-start | bytes 2359296 | tf_op jit(solution)/shard_map/reduce_scatter | solution.py:78
  8.2 6.9 %copy-start.4 = (bf16[4,64,32]{1,0,2:T(4,128)(2,1)}, bf16[4,64,32]{1,0,2:T(4,128)(2,1)S(1)}, u32[]{:S(2)}) copy-start(bf16[4,64,32]{1,0,2:T(4,128)(2,1)S(1)} %reshape.52) | copy-start | bytes 49156
  9.0 6.1 %copy-start.5 = (bf16[4,64,32]{1,0,2:T(4,128)(2,1)}, bf16[4,64,32]{1,0,2:T(4,128)(2,1)S(1)}, u32[]{:S(2)}) copy-start(bf16[4,64,32]{1,0,2:T(4,128)(2,1)S(1)} %reshape.55) | copy-start | bytes 49156
  12.8 2.5 %copy-start.6 = (f32[256,128]{1,0:T(8,128)S(1)}, f32[256,128]{1,0:T(8,128)}, u32[]{:S(2)}) copy-start(f32[256,128]{1,0:T(8,128)} %param.18) | copy-start | bytes 393220
  15.1 0.9 copy-start.7
  15.1 1.0 copy-start.8
  15.1 1.1 copy-start.9
  15.2 180.5 %all-gather.2.cloned.1.call-start = ((), (), s32[]{:S(2)}) async-start(), calls=%async_computation.2 | async-start | bytes 1179648 | tf_op jit(solution)/shard_map/all_gather | solution.py:100
  131.4 32.7 %copy-start.1 = (f32[256,256]{1,0:T(8,128)}, f32[256,256]{1,0:T(8,128)S(1)}, u32[]{:S(2)}) copy-start(f32[256,256]{1,0:T(8,128)S(1)} %copy.52) | copy-start | bytes 786436
  135.1 53.6 %copy-start.2 = (f32[256,256]{1,0:T(8,128)}, f32[256,256]{1,0:T(8,128)S(1)}, u32[]{:S(2)}) copy-start(f32[256,256]{1,0:T(8,128)S(1)} %copy.51) | copy-start | bytes 786436
  135.1 27.4 %copy-start.3 = (f32[256,128]{0,1:T(8,128)S(1)}, f32[256,128]{0,1:T(8,128)}, u32[]{:S(2)}) copy-start(f32[256,128]{0,1:T(8,128)} %get-tuple-element.39) | copy-start | bytes 393220
  137.9 7.8 %collective-permute-start = (bf16[256,256]{1,0:T(8,128)(2,1)S(1)}, bf16[256,256]{1,0:T(8,128)(2,1)S(1)}, u32[]{:S(2)}, u32[]{:S(2)}) collective-permute-start(bf16[256,256]{1,0:T(8,128)(2,1)S(1)} %get-tuple-element.35), channel_id=1, source_target_pairs={{0,4},{4,8},{8,12},{12,16},{16,20},{20,24},{24,28},{28,0},{1,5},{5... | collective-permute-start | bytes 393224 | tf_op jit(solution)/shard_map/ppermute | solution.py:19
  145.7 8.3 %collective-permute-start.1 = (bf16[256,256]{1,0:T(8,128)(2,1)S(1)}, bf16[256,256]{1,0:T(8,128)(2,1)S(1)}, u32[]{:S(2)}, u32[]{:S(2)}) collective-permute-start(bf16[256,256]{1,0:T(8,128)(2,1)S(1)} %collective-permute-done), channel_id=1, source_target_pairs={{0,4},{4,8},{8,12},{12,16},{16,20},{20,24},{24,28},{28,0},{1,5},{5... | collective-permute-start | bytes 393224 | tf_op jit(solution)/shard_map/ppermute | solution.py:19
  154.0 0.7 copy-start.10
  154.6 7.9 %collective-permute-start.2 = (bf16[256,256]{1,0:T(8,128)(2,1)S(1)}, bf16[256,256]{1,0:T(8,128)(2,1)}, u32[]{:S(2)}, u32[]{:S(2)}) collective-permute-start(bf16[256,256]{1,0:T(8,128)(2,1)S(1)} %collective-permute-done.1), channel_id=1, source_target_pairs={{0,4},{4,8},{8,12},{12,16},{16,20},{20,24},{24,28},{28,0},{1,5},{5... | collective-permute-start | bytes 393224 | tf_op jit(solution)/shard_map/ppermute | solution.py:19
  162.5 9.3 %collective-permute-start.3 = (bf16[256,256]{1,0:T(8,128)(2,1)}, bf16[256,256]{1,0:T(8,128)(2,1)}, u32[]{:S(2)}, u32[]{:S(2)}) collective-permute-start(bf16[256,256]{1,0:T(8,128)(2,1)} %collective-permute-done.2), channel_id=1, source_target_pairs={{0,4},{4,8},{8,12},{12,16},{16,20},{20,24},{24,28},{28,0},{1,5},{5... | collective-permute-start | bytes 393224 | tf_op jit(solution)/shard_map/ppermute | solution.py:19
  171.8 7.9 %collective-permute-start.4 = (bf16[256,256]{1,0:T(8,128)(2,1)}, bf16[256,256]{1,0:T(8,128)(2,1)S(1)}, u32[]{:S(2)}, u32[]{:S(2)}) collective-permute-start(bf16[256,256]{1,0:T(8,128)(2,1)} %collective-permute-done.3), channel_id=1, source_target_pairs={{0,4},{4,8},{8,12},{12,16},{16,20},{20,24},{24,28},{28,0},{1,5},{5... | collective-permute-start | bytes 393224 | tf_op jit(solution)/shard_map/ppermute | solution.py:19
  179.7 7.7 %collective-permute-start.5 = (bf16[256,256]{1,0:T(8,128)(2,1)S(1)}, bf16[256,256]{1,0:T(8,128)(2,1)S(1)}, u32[]{:S(2)}, u32[]{:S(2)}) collective-permute-start(bf16[256,256]{1,0:T(8,128)(2,1)S(1)} %collective-permute-done.4), channel_id=1, source_target_pairs={{0,4},{4,8},{8,12},{12,16},{16,20},{20,24},{24,28},{28,0},{1,5},{5... | collective-permute-start | bytes 393224 | tf_op jit(solution)/shard_map/ppermute | solution.py:19
  187.4 7.7 %collective-permute-start.6 = (bf16[256,256]{1,0:T(8,128)(2,1)S(1)}, bf16[256,256]{1,0:T(8,128)(2,1)S(1)}, u32[]{:S(2)}, u32[]{:S(2)}) collective-permute-start(bf16[256,256]{1,0:T(8,128)(2,1)S(1)} %collective-permute-done.5), channel_id=1, source_target_pairs={{0,4},{4,8},{8,12},{12,16},{16,20},{20,24},{24,28},{28,0},{1,5},{5... | collective-permute-start | bytes 393224 | tf_op jit(solution)/shard_map/ppermute | solution.py:19
Sparse Core Ops, SparseCore 0:
  15.3 71.9 reduce-scatter.1
  133.4 42.8 all-gather.1
